TPU v7x, 32 devices: a whole 2x2x4 slice. The times are simulated.
32 devices in a mesh: fs: 4 (over y, x), tp: 8 (over z, core).
Axes of the slice: x: 2, y: 2, z: 4, core: 2. Of those that a mesh axis runs over, the one named last changes fastest.
Arguments:
- stream_in: bfloat16 [4096, 4096], P(('fs', 'tp')), may hold values from -6 to 6
- mixer_out: bfloat16 [4096, 4096], P(('fs', 'tp')), may hold values from -6 to 6
- mix_gain: float32 [4096], replicated, may hold values from 0.1 to 1.9
- pre_gain: float32 [4096], replicated, may hold values from 0.1 to 1.9
- gate_weight: float32 [4096, 6144], P('fs', 'tp'), may hold values from -0.09375 to 0.09375
- up_weight: float32 [4096, 6144], P('fs', 'tp'), may hold values from -0.09375 to 0.09375
- gate_scale: float32 [6144], P('tp'), may hold values from 0.5 to 2
- up_scale: float32 [6144], P('tp'), may hold values from 0.5 to 2
Outputs:
- hidden: bfloat16 [4096, 6144], P('fs', 'tp')
- stream: bfloat16 [4096, 4096], P(('fs', 'tp'))
All inputs are finite; a program needn't handle non-finite values.
Results may differ from a plain program's by a relative error of at most 0.0082.
Values may be sent and summed in bfloat16 or wider, within the bound.
A program may use at most 128 MiB of HBM per device.

v0:
```python
import jax
import jax.numpy as jnp
from jax import lax
from jax.sharding import PartitionSpec as P

epsilon = 1e-06


def rms_scaled(values, gain):
    return values * lax.rsqrt(jnp.mean(values * values, axis=-1, keepdims=True) + epsilon) * gain


def on_device(
    stream_in, mixer_out, mix_gain, pre_gain, gate_weight, up_weight, gate_scale, up_scale
):
    mixed = stream_in.astype(jnp.float32) + rms_scaled(mixer_out.astype(jnp.float32), mix_gain)
    stream = mixed.astype(jnp.bfloat16)
    normed = rms_scaled(stream.astype(jnp.float32), pre_gain).astype(jnp.bfloat16)
    gate_cast = gate_weight.astype(jnp.bfloat16)
    up_cast = up_weight.astype(jnp.bfloat16)
    gate_full, up_full = (
        lax.all_gather(gate_cast, "fs", axis=0, tiled=True),
        lax.all_gather(up_cast, "fs", axis=0, tiled=True),
    )
    piece = lax.all_gather(normed, "tp", axis=0, tiled=True)
    gate = jnp.dot(piece, gate_full, preferred_element_type=jnp.float32) * gate_scale
    up = jnp.dot(piece, up_full, preferred_element_type=jnp.float32) * up_scale
    hidden = (jax.nn.silu(gate) * up).astype(jnp.bfloat16)
    return (hidden, stream)


def solution(mesh):
    return jax.shard_map(
        on_device,
        mesh=mesh,
        in_specs=(
            P(("fs", "tp"), None),
            P(("fs", "tp"), None),
            P(),
            P(),
            P("fs", "tp"),
            P("fs", "tp"),
            P("tp"),
            P("tp"),
        ),
        out_specs=(P("fs", "tp"), P(("fs", "tp"), None)),
        check_vma=False,
    )
```

profile of v0, /device:TPU:0, one launch (start us, length us, event | category | flops | bytes accessed | tf_op | source)
XLA Modules:
  0.0 256.1 jit_solution(6884719773406794379)
XLA Ops:
  7.2 0.0 copy-start.1
  7.2 0.0 copy-start.3
  7.2 0.0 copy-start.2
  7.2 0.0 all-gather.6.cloned.1.call-start
  7.2 3.3 %convert_element_type.29 = bf16[1024,768]{1,0:T(8,128)(2,1)} convert(f32[1024,768]{1,0:T(8,128)} %param.12) | non-fusion elementwise | flops 786432 | bytes 4718592 | tf_op jit(solution)/shard_map/convert_element_type | solution.py:19
  10.6 0.0 copy-start.4
  10.6 0.0 all-gather.6.cloned.1.call-update
  10.6 0.0 all-gather.4.cloned.1.call-start
  10.6 0.0 copy-done.1
  10.6 0.3 fusion
  10.9 0.0 copy-done.3
  11.0 0.0 copy-done.2
  11.0 0.7 fusion.4
  11.7 0.0 copy-start
  11.7 0.0 copy-done.4
  11.7 1.3 fusion.6
  13.1 0.0 all-gather.4.cloned.1.call-update
  13.1 0.0 all-gather.8.cloned.1.call-start
  13.2 3.2 %convert_element_type.30 = bf16[1024,768]{1,0:T(8,128)(2,1)} convert(f32[1024,768]{1,0:T(8,128)} %param.13) | non-fusion elementwise | flops 786432 | bytes 4718592 | tf_op jit(solution)/shard_map/convert_element_type | solution.py:20
  16.4 0.0 copy-done
  16.4 0.0 all-gather.8.cloned.1.call-update
  16.4 0.0 copy-start.5
  16.4 0.0 copy-start.6
  16.4 67.1 %all-gather.6.cloned.1.call-done = bf16[4096,768]{1,0:T(8,128)(2,1)} async-done(((bf16[1024,768]{1,0:T(8,128)(2,1)}), bf16[4096,768]{1,0:T(8,128)(2,1)}) %all-gather.6.cloned.1.call-update) | async-done | bytes 6291472 | tf_op jit(solution)/shard_map/all_gather | solution.py:22
  83.5 83.7 %all-gather.4.cloned.1.call-done = bf16[1024,4096]{1,0:T(8,128)(2,1)} async-done(((bf16[128,4096]{1,0:T(8,128)(2,1)}), bf16[1024,4096]{1,0:T(8,128)(2,1)}) %all-gather.4.cloned.1.call-update) | async-done | bytes 8388624 | tf_op jit(solution)/shard_map/all_gather | solution.py:25
  167.2 10.9 %fusion.8 = f32[1024,768]{1,0:T(8,128)S(1)} fusion(bf16[1024,4096]{1,0:T(8,128)(2,1)} %all-gather.4.cloned.1.call-done, bf16[4096,768]{1,0:T(8,128)(2,1)} %all-gather.6.cloned.1.call-done), kind=kOutput, calls=%fused_computation.14 | convolution fusion | flops 6442450944 | bytes 17825792 | tf_op jit(solution)/shard_map/dot_general | solution.py:26
  178.1 59.5 %all-gather.8.cloned.1.call-done = bf16[4096,768]{1,0:T(8,128)(2,1)} async-done(((bf16[1024,768]{1,0:T(8,128)(2,1)}), bf16[4096,768]{1,0:T(8,128)(2,1)}) %all-gather.8.cloned.1.call-update) | async-done | bytes 6291472 | tf_op jit(solution)/shard_map/all_gather | solution.py:23
  237.6 0.0 copy-done.5
  237.6 0.0 copy-done.6
  237.6 12.1 %multiply_convert_fusion = bf16[1024,768]{1,0:T(8,128)(2,1)} fusion(f32[1024,768]{1,0:T(8,128)S(1)} %fusion.8, bf16[1024,4096]{1,0:T(8,128)(2,1)} %all-gather.4.cloned.1.call-done, bf16[4096,768]{1,0:T(8,128)(2,1)} %all-gather.8.cloned.1.call-done, f32[768]{0:T(1024)S(1)} %copy-done.5, f32[768]{0:T(1024)S(1)} %copy-done.6), kind=kOutput, calls=%fused_computation | convolution fusion | flops 6448742400 | bytes 19404800 | tf_op jit(solution)/shard_map/dot_general | solution.py:27
  (2 shorter events, 0.0 us)
Async XLA Ops:
  7.2 3.5 %copy-start.1 = (bf16[128,4096]{1,0:T(8,128)(2,1)S(1)}, bf16[128,4096]{1,0:T(8,128)(2,1)}, u32[]{:S(2)}) copy-start(bf16[128,4096]{1,0:T(8,128)(2,1)} %param.9) | copy-start | bytes 3145732
  7.2 3.8 %copy-start.3 = (f32[4096]{0:T(1024)S(1)}, f32[4096]{0:T(1024)}, u32[]{:S(2)}) copy-start(f32[4096]{0:T(1024)} %param.10) | copy-start | bytes 49156
  7.2 3.8 %copy-start.2 = (bf16[128,4096]{1,0:T(8,128)(2,1)S(1)}, bf16[128,4096]{1,0:T(8,128)(2,1)}, u32[]{:S(2)}) copy-start(bf16[128,4096]{1,0:T(8,128)(2,1)} %param.8) | copy-start | bytes 3145732
  7.2 76.3 %all-gather.6.cloned.1.call-start = ((), (), s32[]{:S(2)}) async-start(), calls=%async_computation.1 | async-start | bytes 7864320 | tf_op jit(solution)/shard_map/all_gather | solution.py:22
  10.6 1.2 copy-start.4
  10.6 156.6 %all-gather.4.cloned.1.call-start = ((), (), s32[]{:S(2)}) async-start(), calls=%async_computation | async-start | bytes 9437184 | tf_op jit(solution)/shard_map/all_gather | solution.py:25
  11.7 4.7 %copy-start = (bf16[128,4096]{1,0:T(8,128)(2,1)}, bf16[128,4096]{1,0:T(8,128)(2,1)S(1)}, u32[]{:S(2)}) copy-start(bf16[128,4096]{1,0:T(8,128)(2,1)S(1)} %get-tuple-element.3) | copy-start | bytes 3145732
  13.1 224.4 %all-gather.8.cloned.1.call-start = ((), (), s32[]{:S(2)}) async-start(), calls=%async_computation.2 | async-start | bytes 7864320 | tf_op jit(solution)/shard_map/all_gather | solution.py:23
  16.4 221.2 %copy-start.5 = (f32[768]{0:T(1024)S(1)}, f32[768]{0:T(1024)}, u32[]{:S(2)}) copy-start(f32[768]{0:T(1024)} %param.15) | copy-start | bytes 9220
  16.4 221.1 %copy-start.6 = (f32[768]{0:T(1024)S(1)}, f32[768]{0:T(1024)}, u32[]{:S(2)}) copy-start(f32[768]{0:T(1024)} %param.14) | copy-start | bytes 9220
Sparse Core Ops, SparseCore 0:
  10.7 72.7 all-gather.5
  85.1 82.0 all-gather.3
  169.0 68.5 all-gather.7
where the time goes:
time: 256 us
  waiting for transfers between devices  210 us (82%)
  matrix products  23 us (9%)
  between operations  13.8 us (5%)
  other arithmetic  8.92 us (3%)
    all_gather x1, waiting for transfers between devices, on_device(): piece = lax.all_gather(normed, 'tp', axis=0, tiled=True)  83.7 us
    all_gather x1, waiting for transfers between devices, on_device(): lax.all_gather(gate_cast, 'fs', axis=0, tiled=True)  67.1 us
    all_gather x1, waiting for transfers between devices, on_device(): lax.all_gather(up_cast, 'fs', axis=0, tiled=True)  59.5 us
    dot_general x1, matrix products, on_device(): up = jnp.dot(piece, up_full, preferred_element_type=jnp.float32) * up_scale  12.1 us
    dot_general x1, matrix products, on_device(): jnp.dot(piece, gate_full, preferred_element_type=jnp.float32) * gate_scale  10.9 us
  transfers between devices with their start and end apart: 3, of which 3 were waited for; matrix products, arithmetic and copies ran while one was open for 6% of the time, Pallas kernels for 0%

commit v1 on v0

--- a/solution.py
+++ b/solution.py
@@ -4,6 +4,16 @@
 from jax.sharding import PartitionSpec as P
 
 epsilon = 1e-06
+
+
+def pass_along(value, name, dim):
+    size = lax.axis_size(name)
+    moving, blocks = (value, [value])
+    for _ in range(size - 1):
+        moving = lax.ppermute(moving, name, [(i, (i + 1) % size) for i in range(size)])
+        blocks.insert(0, moving)
+    line = jnp.concatenate(blocks, axis=dim)
+    return jnp.roll(line, (lax.axis_index(name) + 1) * value.shape[dim], axis=dim)
 
 
 def rms_scaled(values, gain):
@@ -22,7 +32,7 @@
         lax.all_gather(gate_cast, "fs", axis=0, tiled=True),
         lax.all_gather(up_cast, "fs", axis=0, tiled=True),
     )
-    piece = lax.all_gather(normed, "tp", axis=0, tiled=True)
+    piece = pass_along(normed, "tp", 0)
     gate = jnp.dot(piece, gate_full, preferred_element_type=jnp.float32) * gate_scale
     up = jnp.dot(piece, up_full, preferred_element_type=jnp.float32) * up_scale
     hidden = (jax.nn.silu(gate) * up).astype(jnp.bfloat16)

time: 256 us -> 208 us (0.81)
  waiting for transfers between devices: 210 us -> 132 us
  local copies, waits for them, and re-layouts: 0.04 us -> 25.7 us
  other arithmetic: 8.92 us -> 11.6 us
    ppermute x0 -> x7, waiting for transfers between devices: none -> 112 us  [pass_along(): lax.ppermute(moving, name, [(i, (i + 1) % size) for i in range(size)])]
    all_gather x1 -> x0, waiting for transfers between devices: 83.7 us -> none  [on_device(): piece = lax.all_gather(normed, 'tp', axis=0, tiled=True)]
    all_gather x1, waiting for transfers between devices: 67.1 us -> 0.01 us  [on_device(): lax.all_gather(gate_cast, 'fs', axis=0, tiled=True)]
    all_gather x1, waiting for transfers between devices: 59.5 us -> 20.6 us  [on_device(): lax.all_gather(up_cast, 'fs', axis=0, tiled=True)]
    unnamed x14 -> x36, local copies, waits for them, and re-layouts: 0.04 us -> 25.7 us
    reduce_sum x2, other arithmetic: 1.03 us -> 3.97 us  [rms_scaled(): jnp.mean(values * values, axis=-1, keepdims=True) + epsilon]
  transfers between devices with their start and end apart: 3 -> 9, of which waited for: 3 -> 8; matrix products, arithmetic and copies ran while one was open for 6% -> 20% of each run, Pallas kernels for 0% -> 0%
where the time goes in v1:
time: 208 us; the launch traced here: 207 us
  waiting for transfers between devices  132 us (63%)
  local copies, waits for them, and re-layouts  25.7 us (12%)
  matrix products  23 us (11%)
  between operations  14.1 us (7%)
  other arithmetic  11.6 us (6%)
    ppermute x7, waiting for transfers between devices, pass_along(): lax.ppermute(moving, name, [(i, (i + 1) % size) for i in range(size)])  112 us
    unnamed x36, local copies, waits for them, and re-layouts  25.7 us
    all_gather x1, waiting for transfers between devices, on_device(): lax.all_gather(up_cast, 'fs', axis=0, tiled=True)  20.6 us
    dot_general x1, matrix products, on_device(): up = jnp.dot(piece, up_full, preferred_element_type=jnp.float32) * up_scale  12.1 us
    dot_general x1, matrix products, on_device(): jnp.dot(piece, gate_full, preferred_element_type=jnp.float32) * gate_scale  10.9 us
  transfers between devices with their start and end apart: 9, of which 8 were waited for; matrix products, arithmetic and copies ran while one was open for 20% of the time, Pallas kernels for 0%

profile of v1, /device:TPU:0, one launch (start us, length us, event | category | flops | bytes accessed | tf_op | source)
XLA Modules:
  0.0 207.3 jit_solution(7376714745754712901)
XLA Ops:
  7.2 0.0 copy-start.8
  7.2 0.0 all-gather.3.cloned.1.call-start
  7.2 3.2 %convert_element_type.29 = bf16[1024,768]{1,0:T(8,128)(2,1)} convert(f32[1024,768]{1,0:T(8,128)} %param.12) | non-fusion elementwise | flops 786432 | bytes 4718592 | tf_op jit(solution)/shard_map/convert_element_type | solution.py:29
  10.4 0.0 all-gather.3.cloned.1.call-update
  10.4 0.0 all-gather.5.cloned.1.call-start
  10.5 0.0 copy-start.7
  10.5 1.7 fusion.4
  12.2 2.3 %fusion.8 = (f32[128]{0:T(128)S(1)}, bf16[128,4096]{1,0:T(8,128)(2,1)S(1)}) fusion(f32[4096]{0:T(1024)} %param.10, f32[128]{0:T(128)S(1)} %add_rsqrt_fusion.1, bf16[128,4096]{1,0:T(8,128)(2,1)} %param.9, bf16[128,4096]{1,0:T(8,128)(2,1)} %param.8), kind=kLoop, calls=%fused_computation.13 | loop fusion | flops 4718464 | bytes 3163136 | tf_op jit(solution)/shard_map/reduce_sum | solution.py:20
  14.5 0.0 copy-start
  14.5 0.3 fusion.10
  14.9 0.5 collective-permute-start
  15.4 16.5 %collective-permute-done = bf16[128,4096]{1,0:T(8,128)(2,1)S(1)} collective-permute-done((bf16[128,4096]{1,0:T(8,128)(2,1)S(1)}, bf16[128,4096]{1,0:T(8,128)(2,1)S(1)}, u32[]{:S(2)}, u32[]{:S(2)}) %collective-permute-start) | collective-permute-done | bytes 1048608 | tf_op jit(solution)/shard_map/ppermute | solution.py:13
  31.9 0.0 collective-permute-start.1
  31.9 16.0 %collective-permute-done.1 = bf16[128,4096]{1,0:T(8,128)(2,1)S(1)} collective-permute-done((bf16[128,4096]{1,0:T(8,128)(2,1)S(1)}, bf16[128,4096]{1,0:T(8,128)(2,1)S(1)}, u32[]{:S(2)}, u32[]{:S(2)}) %collective-permute-start.1) | collective-permute-done | bytes 1048608 | tf_op jit(solution)/shard_map/ppermute | solution.py:13
  47.9 0.0 collective-permute-start.2
  47.9 16.0 %collective-permute-done.2 = bf16[128,4096]{1,0:T(8,128)(2,1)S(1)} collective-permute-done((bf16[128,4096]{1,0:T(8,128)(2,1)S(1)}, bf16[128,4096]{1,0:T(8,128)(2,1)S(1)}, u32[]{:S(2)}, u32[]{:S(2)}) %collective-permute-start.2) | collective-permute-done | bytes 1048608 | tf_op jit(solution)/shard_map/ppermute | solution.py:13
  64.0 1.0 copy-done.1
  64.9 0.0 collective-permute-start.3
  64.9 16.0 %collective-permute-done.3 = bf16[128,4096]{1,0:T(8,128)(2,1)S(1)} collective-permute-done((bf16[128,4096]{1,0:T(8,128)(2,1)S(1)}, bf16[128,4096]{1,0:T(8,128)(2,1)S(1)}, u32[]{:S(2)}, u32[]{:S(2)}) %collective-permute-start.3) | collective-permute-done | bytes 1048608 | tf_op jit(solution)/shard_map/ppermute | solution.py:13
  81.0 1.0 copy-done.3
  81.9 0.0 collective-permute-start.4
  81.9 16.0 %collective-permute-done.4 = bf16[128,4096]{1,0:T(8,128)(2,1)S(1)} collective-permute-done((bf16[128,4096]{1,0:T(8,128)(2,1)S(1)}, bf16[128,4096]{1,0:T(8,128)(2,1)S(1)}, u32[]{:S(2)}, u32[]{:S(2)}) %collective-permute-start.4) | collective-permute-done | bytes 1048608 | tf_op jit(solution)/shard_map/ppermute | solution.py:13
  97.9 1.0 copy-done.5
  98.9 0.0 collective-permute-start.5
  98.9 16.1 %collective-permute-done.5 = bf16[128,4096]{1,0:T(8,128)(2,1)} collective-permute-done((bf16[128,4096]{1,0:T(8,128)(2,1)S(1)}, bf16[128,4096]{1,0:T(8,128)(2,1)}, u32[]{:S(2)}, u32[]{:S(2)}) %collective-permute-start.5) | collective-permute-done | bytes 1048608 | tf_op jit(solution)/shard_map/ppermute | solution.py:13
  115.1 0.0 collective-permute-start.6
  115.1 1.4 convert_element_type.30
  116.4 0.0 all-gather.5.cloned.1.call-update
  116.5 14.9 %collective-permute-done.6 = bf16[128,4096]{1,0:T(8,128)(2,1)} collective-permute-done((bf16[128,4096]{1,0:T(8,128)(2,1)}, bf16[128,4096]{1,0:T(8,128)(2,1)}, u32[]{:S(2)}, u32[]{:S(2)}) %collective-permute-start.6) | collective-permute-done | bytes 1048608 | tf_op jit(solution)/shard_map/ppermute | solution.py:13
  131.4 2.3 %constant_dynamic-update-slice_fusion.15 = bf16[2048,4096]{1,0:T(8,128)(2,1)} fusion(bf16[128,4096]{1,0:T(8,128)(2,1)} %collective-permute-done.6), kind=kLoop, calls=%fused_computation.31 | loop fusion | bytes 2097152
  133.7 2.3 %constant_dynamic-update-slice_fusion.14 = bf16[2048,4096]{1,0:T(8,128)(2,1)} fusion(bf16[2048,4096]{1,0:T(8,128)(2,1)} %constant_dynamic-update-slice_fusion.15, bf16[128,4096]{1,0:T(8,128)(2,1)} %collective-permute-done.5), kind=kLoop, calls=%fused_computation.30 | loop fusion | bytes 2097152
  136.0 2.4 %constant_dynamic-update-slice_fusion.13 = bf16[2048,4096]{1,0:T(8,128)(2,1)} fusion(bf16[2048,4096]{1,0:T(8,128)(2,1)} %constant_dynamic-update-slice_fusion.14, bf16[128,4096]{1,0:T(8,128)(2,1)} %copy-done.5), kind=kLoop, calls=%fused_computation.29 | loop fusion | bytes 2097152
  138.4 2.4 %constant_dynamic-update-slice_fusion.12 = bf16[2048,4096]{1,0:T(8,128)(2,1)} fusion(bf16[2048,4096]{1,0:T(8,128)(2,1)} %constant_dynamic-update-slice_fusion.13, bf16[128,4096]{1,0:T(8,128)(2,1)} %copy-done.3), kind=kLoop, calls=%fused_computation.28 | loop fusion | bytes 2097152
  140.8 1.1 constant_dynamic-update-slice_fusion.11
  141.8 1.1 constant_dynamic-update-slice_fusion.10
  142.9 1.1 constant_dynamic-update-slice_fusion.9
  144.0 1.4 constant_dynamic-update-slice_fusion.8
  145.4 2.4 %constant_dynamic-update-slice_fusion.7 = bf16[2048,4096]{1,0:T(8,128)(2,1)} fusion(bf16[2048,4096]{1,0:T(8,128)(2,1)} %constant_dynamic-update-slice_fusion.8, bf16[128,4096]{1,0:T(8,128)(2,1)} %collective-permute-done.6), kind=kLoop, calls=%fused_computation.23 | loop fusion | bytes 2097152
  147.8 2.3 %constant_dynamic-update-slice_fusion.6 = bf16[2048,4096]{1,0:T(8,128)(2,1)} fusion(bf16[2048,4096]{1,0:T(8,128)(2,1)} %constant_dynamic-update-slice_fusion.7, bf16[128,4096]{1,0:T(8,128)(2,1)} %collective-permute-done.5), kind=kLoop, calls=%fused_computation.22 | loop fusion | bytes 2097152
  150.1 1.1 constant_dynamic-update-slice_fusion.5
  151.2 1.1 constant_dynamic-update-slice_fusion.4
  152.3 1.1 constant_dynamic-update-slice_fusion.3
  153.4 1.1 constant_dynamic-update-slice_fusion.2
  154.4 1.1 constant_dynamic-update-slice_fusion.1
  155.5 1.3 constant_dynamic-update-slice_fusion
  156.8 10.9 %fusion.2 = f32[1024,768]{1,0:T(8,128)S(1)} fusion(bf16[4096,768]{1,0:T(8,128)(2,1)} %all-gather.3.cloned.1.call-done, bf16[2048,4096]{1,0:T(8,128)(2,1)} %constant_dynamic-update-slice_fusion, s32[]{:T(128)S(6)} %select_n.14), kind=kOutput, calls=%fused_computation.2 | convolution fusion | flops 6442450944 | bytes 17825796 | tf_op jit(solution)/shard_map/dot_general | solution.py:36
  167.8 20.6 %all-gather.5.cloned.1.call-done = bf16[4096,768]{1,0:T(8,128)(2,1)} async-done(((bf16[1024,768]{1,0:T(8,128)(2,1)}), bf16[4096,768]{1,0:T(8,128)(2,1)}) %all-gather.5.cloned.1.call-update) | async-done | bytes 6291472 | tf_op jit(solution)/shard_map/all_gather | solution.py:33
  188.3 12.1 %multiply_convert_fusion = bf16[1024,768]{1,0:T(8,128)(2,1)} fusion(f32[1024,768]{1,0:T(8,128)S(1)} %fusion.2, bf16[4096,768]{1,0:T(8,128)(2,1)} %all-gather.5.cloned.1.call-done, bf16[2048,4096]{1,0:T(8,128)(2,1)} %constant_dynamic-update-slice_fusion, s32[]{:T(128)S(6)} %select_n.14, f32[768]{0:T(1024)S(1)} %copy-done.9, f32[768]{0:T(1024)S(1)} %copy-done.10), kind=kOutput, calls=%fused_computation.4 | convolution fusion | flops 6448742400 | bytes 19404804 | tf_op jit(solution)/shard_map/dot_general | solution.py:37
  (19 shorter events, 0.0 us)
Async XLA Ops:
  7.2 7.3 %copy-start.8 = (f32[4096]{0:T(1024)S(1)}, f32[4096]{0:T(1024)}, u32[]{:S(2)}) copy-start(f32[4096]{0:T(1024)} %param.11) | copy-start | bytes 49156
  7.2 149.7 %all-gather.3.cloned.1.call-start = ((), (), s32[]{:S(2)}) async-start(), calls=%async_computation | async-start | bytes 7864320 | tf_op jit(solution)/shard_map/all_gather | solution.py:32
  10.4 177.9 %all-gather.5.cloned.1.call-start = ((), (), s32[]{:S(2)}) async-start(), calls=%async_computation.1 | async-start | bytes 7864320 | tf_op jit(solution)/shard_map/all_gather | solution.py:33
  10.5 104.6 %copy-start.7 = (f32[1024,768]{1,0:T(8,128)S(1)}, f32[1024,768]{1,0:T(8,128)}, u32[]{:S(2)}) copy-start(f32[1024,768]{1,0:T(8,128)} %param.13) | copy-start | bytes 9437188
  14.5 141.0 %copy-start = (bf16[128,4096]{1,0:T(8,128)(2,1)}, bf16[128,4096]{1,0:T(8,128)(2,1)S(1)}, u32[]{:S(2)}) copy-start(bf16[128,4096]{1,0:T(8,128)(2,1)S(1)} %get-tuple-element.3) | copy-start | bytes 3145732
  14.9 17.1 %collective-permute-start = (bf16[128,4096]{1,0:T(8,128)(2,1)S(1)}, bf16[128,4096]{1,0:T(8,128)(2,1)S(1)}, u32[]{:S(2)}, u32[]{:S(2)}) collective-permute-start(bf16[128,4096]{1,0:T(8,128)(2,1)S(1)} %fusion.10), channel_id=1, source_target_pairs={{0,1},{1,2},{2,3},{3,4},{4,5},{5,6},{6,7},{7,0},{8,9},{9,10},{10,1... | collective-permute-start | bytes 3145736 | tf_op jit(solution)/shard_map/ppermute | solution.py:13
  31.9 16.0 %collective-permute-start.1 = (bf16[128,4096]{1,0:T(8,128)(2,1)S(1)}, bf16[128,4096]{1,0:T(8,128)(2,1)S(1)}, u32[]{:S(2)}, u32[]{:S(2)}) collective-permute-start(bf16[128,4096]{1,0:T(8,128)(2,1)S(1)} %collective-permute-done), channel_id=1, source_target_pairs={{0,1},{1,2},{2,3},{3,4},{4,5},{5,6},{6,7},{7,0},{8,9},{9,10},{10,1... | collective-permute-start | bytes 3145736 | tf_op jit(solution)/shard_map/ppermute | solution.py:13
  47.9 16.0 %collective-permute-start.2 = (bf16[128,4096]{1,0:T(8,128)(2,1)S(1)}, bf16[128,4096]{1,0:T(8,128)(2,1)S(1)}, u32[]{:S(2)}, u32[]{:S(2)}) collective-permute-start(bf16[128,4096]{1,0:T(8,128)(2,1)S(1)} %collective-permute-done.1), channel_id=1, source_target_pairs={{0,1},{1,2},{2,3},{3,4},{4,5},{5,6},{6,7},{7,0},{8,9},{9,10},{10,1... | collective-permute-start | bytes 3145736 | tf_op jit(solution)/shard_map/ppermute | solution.py:13
  64.0 1.0 copy-start.1
  64.9 16.0 %collective-permute-start.3 = (bf16[128,4096]{1,0:T(8,128)(2,1)S(1)}, bf16[128,4096]{1,0:T(8,128)(2,1)S(1)}, u32[]{:S(2)}, u32[]{:S(2)}) collective-permute-start(bf16[128,4096]{1,0:T(8,128)(2,1)S(1)} %collective-permute-done.2), channel_id=1, source_target_pairs={{0,1},{1,2},{2,3},{3,4},{4,5},{5,6},{6,7},{7,0},{8,9},{9,10},{10,1... | collective-permute-start | bytes 3145736 | tf_op jit(solution)/shard_map/ppermute | solution.py:13
  81.0 1.0 copy-start.3
  81.9 16.0 %collective-permute-start.4 = (bf16[128,4096]{1,0:T(8,128)(2,1)S(1)}, bf16[128,4096]{1,0:T(8,128)(2,1)S(1)}, u32[]{:S(2)}, u32[]{:S(2)}) collective-permute-start(bf16[128,4096]{1,0:T(8,128)(2,1)S(1)} %collective-permute-done.3), channel_id=1, source_target_pairs={{0,1},{1,2},{2,3},{3,4},{4,5},{5,6},{6,7},{7,0},{8,9},{9,10},{10,1... | collective-permute-start | bytes 3145736 | tf_op jit(solution)/shard_map/ppermute | solution.py:13
  97.9 1.0 copy-start.5
  98.9 16.1 %collective-permute-start.5 = (bf16[128,4096]{1,0:T(8,128)(2,1)S(1)}, bf16[128,4096]{1,0:T(8,128)(2,1)}, u32[]{:S(2)}, u32[]{:S(2)}) collective-permute-start(bf16[128,4096]{1,0:T(8,128)(2,1)S(1)} %collective-permute-done.4), channel_id=1, source_target_pairs={{0,1},{1,2},{2,3},{3,4},{4,5},{5,6},{6,7},{7,0},{8,9},{9,10},{10,1... | collective-permute-start | bytes 3145736 | tf_op jit(solution)/shard_map/ppermute | solution.py:13
  115.1 16.3 %collective-permute-start.6 = (bf16[128,4096]{1,0:T(8,128)(2,1)}, bf16[128,4096]{1,0:T(8,128)(2,1)}, u32[]{:S(2)}, u32[]{:S(2)}) collective-permute-start(bf16[128,4096]{1,0:T(8,128)(2,1)} %collective-permute-done.5), channel_id=1, source_target_pairs={{0,1},{1,2},{2,3},{3,4},{4,5},{5,6},{6,7},{7,0},{8,9},{9,10},{10,1... | collective-permute-start | bytes 3145736 | tf_op jit(solution)/shard_map/ppermute | solution.py:13
  116.5 24.3 %copy-start.2 = (bf16[128,4096]{1,0:T(8,128)(2,1)S(1)}, bf16[128,4096]{1,0:T(8,128)(2,1)}, u32[]{:S(2)}) copy-start(bf16[128,4096]{1,0:T(8,128)(2,1)} %copy-done.1) | copy-start | bytes 3145732
  136.0 14.1 %copy-start.6 = (bf16[128,4096]{1,0:T(8,128)(2,1)S(1)}, bf16[128,4096]{1,0:T(8,128)(2,1)}, u32[]{:S(2)}) copy-start(bf16[128,4096]{1,0:T(8,128)(2,1)} %copy-done.5) | copy-start | bytes 3145732
  138.4 12.8 %copy-start.4 = (bf16[128,4096]{1,0:T(8,128)(2,1)S(1)}, bf16[128,4096]{1,0:T(8,128)(2,1)}, u32[]{:S(2)}) copy-start(bf16[128,4096]{1,0:T(8,128)(2,1)} %copy-done.3) | copy-start | bytes 3145732
  156.8 31.5 %copy-start.9 = (f32[768]{0:T(1024)S(1)}, f32[768]{0:T(1024)}, u32[]{:S(2)}) copy-start(f32[768]{0:T(1024)} %param.15) | copy-start | bytes 9220
  156.8 31.5 %copy-start.10 = (f32[768]{0:T(1024)S(1)}, f32[768]{0:T(1024)}, u32[]{:S(2)}) copy-start(f32[768]{0:T(1024)} %param.14) | copy-start | bytes 9220
Sparse Core Ops, SparseCore 0:
  10.6 72.7 all-gather.2
  116.6 71.7 all-gather.4
